TPU v7x, 32 devices: a whole 2x2x4 slice. The times are simulated.
32 devices in a mesh: ep: 4 (over y, x), tp: 8 (over z, core).
Axes of the slice: x: 2, y: 2, z: 4, core: 2. Of those that a mesh axis runs over, the one named last changes fastest.
Arguments:
- queries: bfloat16 [4096, 1024], P('ep', 'tp'), may hold values from -8 to 8
- keys: bfloat16 [4096, 256], P('ep'), may hold values from -8 to 8
- values: bfloat16 [4096, 256], P('ep'), may hold values from -6 to 6
- query_gain: float32 [64], replicated, may hold values from 1 to 10
- key_gain: float32 [64], replicated, may hold values from 1 to 10
- moe_input: bfloat16 [1536, 2048], P(('ep', 'tp')), may hold values from -6 to 6
- expert_ids: int32 [1536, 2], P('ep'), may hold values from 0 to 3, all different within a row; in each aligned block of 48 rows (0 to 47, 48 to 95, ...) at most 30 rows name the same one
- route_weight: float32 [1536, 2], P('ep'), may hold values from 0.2 to 1
- gate_weight: bfloat16 [4, 2048, 7168], P('ep', None, 'tp'), may hold values from -0.125 to 0.125
- up_weight: bfloat16 [4, 2048, 7168], P('ep', None, 'tp'), may hold values from -0.125 to 0.125
- down_weight: bfloat16 [4, 7168, 2048], P('ep', 'tp'), may hold values from -0.0625 to 0.0625
- output_gain: float32 [2048], replicated, may hold values from 0.1 to 1.9
Outputs:
- attended: bfloat16 [4096, 1024], P('ep', 'tp')
- moe_output: bfloat16 [1536, 2048], P(('ep', 'tp'))
Inputs may be any that keep to these rules, and one draw needn't show every extreme that they name: `expert_ids`: the 2 experts of a token differ. In the rows of one device (aligned blocks of 48 tokens) no expert is named by more than 30 tokens, and in every draw some expert is named by exactly 30 tokens of some device.
All inputs are finite; a program needn't handle non-finite values.
Results may differ from a plain program's by a relative error of at most 0.0085.
The roundings to bfloat16 on the way count: a program that leaves them out, or rounds other values in their place, can miss the bound.
Values may be sent and summed in bfloat16 or wider, within the bound.
A program may use at most 128 MiB of HBM per device.

v0:
```python
import math
import jax
import jax.numpy as jnp
from jax import lax
from jax.sharding import PartitionSpec as P

QH = 16
KV = 4
GRID_W = 64
rope_theta = 10000.0
rms_epsilon = 1e-06
norm_epsilon = 1e-05
residual_scale = 1.4142135623730951


def unit_heads(heads, gain_vector):
    squares = jnp.mean(heads * heads, axis=-1, keepdims=True)
    return heads * lax.rsqrt(squares + rms_epsilon) * gain_vector


def rotate_grid(heads, first_position, grid_width):
    head_size = heads.shape[-1]
    pair_count = head_size // 4
    position = first_position + jnp.arange(heads.shape[1], dtype=jnp.int32)
    grid_row = (position // grid_width).astype(jnp.float32)
    grid_col = (position % grid_width).astype(jnp.float32)
    inverse = rope_theta ** (-jnp.arange(pair_count, dtype=jnp.float32) / pair_count)
    angles = jnp.concatenate([grid_row[:, None] * inverse, grid_col[:, None] * inverse], axis=-1)
    cosines = jnp.cos(angles)
    sines = jnp.sin(angles)
    half_size = head_size // 2
    first_half = heads[..., :half_size]
    second_half = heads[..., half_size:]
    return jnp.concatenate(
        [first_half * cosines - second_half * sines, second_half * cosines + first_half * sines],
        axis=-1,
    )


def place_rank(choices, expert_count):
    matches = (choices[..., None] == jnp.arange(expert_count, dtype=jnp.int32)).astype(jnp.int32)
    earlier = jnp.cumsum(matches, axis=1) - matches
    return jnp.sum(earlier * matches, axis=-1)


def shards(
    queries,
    keys,
    values,
    query_gain,
    key_gain,
    moe_input,
    expert_ids,
    route_weight,
    gate_weight,
    up_weight,
    down_weight,
    output_gain,
):
    seg_rows = queries.shape[0]
    head_size = query_gain.shape[0]
    local_heads = queries.shape[1] // head_size
    offset = lax.axis_index("ep") * seg_rows
    key_head = lax.axis_index("tp") * local_heads // (QH // KV)
    key_cols = lax.dynamic_slice_in_dim(keys, key_head * head_size, head_size, 1)
    value_cols = lax.dynamic_slice_in_dim(values, key_head * head_size, head_size, 1)
    query_heads = (
        queries.reshape(seg_rows, local_heads, head_size).transpose(1, 0, 2).astype(jnp.float32)
    )
    rotated_queries = rotate_grid(unit_heads(query_heads, query_gain), offset, GRID_W).astype(
        jnp.bfloat16
    )
    key_heads = key_cols.astype(jnp.float32)[None]
    rotated_keys = rotate_grid(unit_heads(key_heads, key_gain), offset, GRID_W)[0].astype(
        jnp.bfloat16
    )
    score_scale = head_size ** (-0.5)
    initial = (
        jnp.full((local_heads, seg_rows), -jnp.inf, jnp.float32),
        jnp.zeros((local_heads, seg_rows), jnp.float32),
        jnp.zeros((local_heads, head_size, seg_rows), jnp.float32),
    )
    key_piece = lax.all_gather(rotated_keys, "ep", axis=0, tiled=True)
    value_piece = lax.all_gather(value_cols, "ep", axis=0, tiled=True)
    piece_rows = key_piece.shape[0]
    block_rows = math.gcd(piece_rows, 1024)
    key_blocks = key_piece.reshape(piece_rows // block_rows, block_rows, head_size)
    value_blocks = value_piece.reshape(piece_rows // block_rows, block_rows, head_size)

    def sweep(state_now, blocks):
        running_max, row_total, summed = state_now
        key_block, value_block = blocks
        scores = (
            jnp.einsum(
                "hqd,kd->hqk", rotated_queries, key_block, preferred_element_type=jnp.float32
            )
            * score_scale
        )
        new_max = jnp.maximum(running_max, jnp.max(scores, axis=-1))
        shrink = jnp.exp(running_max - new_max)
        weights = jnp.exp(scores - new_max[..., None])
        row_total = row_total * shrink + jnp.sum(weights, axis=-1)
        added = jnp.einsum(
            "hqk,kd->hdq",
            weights.astype(jnp.bfloat16),
            value_block,
            preferred_element_type=jnp.float32,
        )
        summed = summed * shrink[:, None, :] + added
        return ((new_max, row_total, summed), None)

    result, ignored = lax.scan(sweep, initial, (key_blocks, value_blocks))
    row_max, row_total, summed = result
    attended = (
        (summed / row_total[:, None, :])
        .transpose(2, 0, 1)
        .reshape(seg_rows, local_heads * head_size)
        .astype(jnp.bfloat16)
    )
    tok_rows = moe_input.shape[0]
    model_width = moe_input.shape[1]
    top_count = expert_ids.shape[1]
    experts = lax.axis_size("ep")
    capacity = max(2, tok_rows * top_count * 5 // (4 * experts))
    column_index = lax.axis_index("tp")
    own_ids = lax.dynamic_slice_in_dim(expert_ids, column_index * tok_rows, tok_rows, 0).reshape(-1)
    own_weights = lax.dynamic_slice_in_dim(route_weight, column_index * tok_rows, tok_rows, 0)
    own_rank = place_rank(own_ids[None], experts)[0]
    own_slots = own_ids * capacity + own_rank
    token_of = jnp.arange(tok_rows * top_count, dtype=jnp.int32) // top_count
    sources = jnp.full((experts * capacity,), tok_rows, jnp.int32).at[own_slots].set(token_of)
    outgoing = jnp.take(moe_input, sources, axis=0, mode="fill", fill_value=0)
    arrived = lax.all_to_all(
        outgoing.reshape(experts, capacity, model_width),
        "ep",
        split_axis=0,
        concat_axis=0,
        tiled=True,
    )
    shard_piece = lax.all_gather(arrived.reshape(-1, model_width), "tp", axis=0, tiled=True)
    gate_part = jnp.dot(shard_piece, gate_weight[0], preferred_element_type=jnp.float32)
    up_part = jnp.dot(shard_piece, up_weight[0], preferred_element_type=jnp.float32)
    hidden = (jax.nn.silu(gate_part) * up_part).astype(jnp.bfloat16)
    expert_out = lax.psum_scatter(
        jnp.dot(hidden, down_weight[0], preferred_element_type=jnp.float32).astype(jnp.bfloat16),
        "tp",
        scatter_dimension=0,
        tiled=True,
    )
    returned = lax.all_to_all(
        expert_out.reshape(experts, capacity, model_width),
        "ep",
        split_axis=0,
        concat_axis=0,
        tiled=True,
    )
    picked = jnp.take(returned.reshape(experts * capacity, model_width), own_slots, axis=0)
    picked = picked.reshape(tok_rows, top_count, model_width).astype(jnp.float32)
    mixed = residual_scale * moe_input.astype(jnp.float32) + jnp.sum(
        own_weights[:, :, None] * picked, axis=1
    )
    average = jnp.mean(mixed, axis=-1, keepdims=True)
    centered = mixed - average
    variance = jnp.mean(centered * centered, axis=-1, keepdims=True)
    moe_output = (centered * lax.rsqrt(variance + norm_epsilon) * output_gain).astype(jnp.bfloat16)
    return (attended, moe_output)


def solution(mesh):
    in_specs = (
        P("ep", "tp"),
        P("ep", None),
        P("ep", None),
        P(),
        P(),
        P(("ep", "tp"), None),
        P("ep", None),
        P("ep", None),
        P("ep", None, "tp"),
        P("ep", None, "tp"),
        P("ep", "tp", None),
        P(),
    )
    out_specs = (P("ep", "tp"), P(("ep", "tp"), None))
    return jax.shard_map(shards, mesh=mesh, in_specs=in_specs, out_specs=out_specs, check_vma=False)
```

profile of v0, /device:TPU:0, one launch (start us, length us, event | category | flops | bytes accessed | tf_op | source)
XLA Modules:
  0.0 168.1 jit_solution(6163378667000883554)
XLA Ops:
  8.9 0.9 scatter_custom_fusion
  9.8 2.3 %gather_fusion = bf16[120,2048]{1,0:T(8,128)(2,1)S(1)} fusion(bf16[48,2048]{1,0:T(8,128)(2,1)} %param.19, s32[1024]{0:T(1024)S(1)} %pad_clamp_fusion.1), kind=kCustom, calls=%fused_computation | custom fusion | bytes 983520 | tf_op jit(solution)/shard_map/jit(_take)/gather | solution.py:132
  12.5 13.6 %all_to_all.10 = bf16[4,30,2048]{2,1,0:T(8,128)(2,1)S(1)} all-to-all(bf16[4,30,2048]{2,1,0:T(8,128)(2,1)S(1)} %broadcast_select_fusion.2), channel_id=1, replica_groups=mesh['ep'=4,'tp'=8] {'ep'}, dimensions={0} | all-to-all | bytes 983040 | tf_op jit(solution)/shard_map/all_to_all | solution.py:133
  26.2 0.9 reshape.418
  28.5 10.1 %all-gather = bf16[1,4096,64]{1,2,0:T(8,128)(2,1)S(1)} all-gather(bf16[1,1024,64]{1,2,0:T(8,128)(2,1)S(1)} %pad_maximum_fusion.2), channel_id=2, replica_groups=mesh['ep'=4,'tp'=8] {'ep'}, dimensions={1}, use_global_device_ids=true | all-gather | bytes 655360 | tf_op jit(solution)/shard_map/all_gather | solution.py:83
  39.0 1.0 copy.45
  40.3 13.1 %all_gather.10 = bf16[4096,64]{1,0:T(8,128)(2,1)S(1)} all-gather(bf16[1024,64]{1,0:T(8,128)(2,1)S(1)} %constant_dynamic-slice_fusion.2), channel_id=1, replica_groups=mesh['ep'=4,'tp'=8] {'ep'}, dimensions={0}, use_global_device_ids=true | all-gather | bytes 655360 | tf_op jit(solution)/shard_map/all_gather | solution.py:84
  54.5 17.2 %all-gather.3.cloned.1.call-done = bf16[960,2048]{1,0:T(8,128)(2,1)} async-done(((bf16[120,2048]{1,0:T(8,128)(2,1)}), bf16[960,2048]{1,0:T(8,128)(2,1)}) %all-gather.3.cloned.1.call-update) | async-done | bytes 3932176 | tf_op jit(solution)/shard_map/all_gather | solution.py:140
  71.7 7.6 %fusion.22 = f32[960,896]{1,0:T(8,128)S(1)} fusion(bf16[960,2048]{1,0:T(8,128)(2,1)} %all-gather.3.cloned.1.call-done, bf16[1,2048,896]{2,1,0:T(8,128)(2,1)} %param.23), kind=kOutput, calls=%fused_computation.27 | convolution fusion | flops 3523215360 | bytes 11042816 | tf_op jit(solution)/shard_map/dot_general | solution.py:142
  79.3 4.5 %multiply_convert_fusion = bf16[960,896]{1,0:T(8,128)(2,1)S(1)} fusion(f32[960,896]{1,0:T(8,128)S(1)} %fusion.22, bf16[960,2048]{1,0:T(8,128)(2,1)S(1)} %copy-done.8, bf16[1,2048,896]{2,1,0:T(8,128)(2,1)S(1)} %copy-done.9), kind=kOutput, calls=%fused_computation.31 | convolution fusion | flops 3528376320 | bytes 12763136 | tf_op jit(solution)/shard_map/dot_general | solution.py:141
  83.8 5.9 %convolution_convert_fusion = bf16[960,2048]{1,0:T(8,128)(2,1)} fusion(bf16[960,896]{1,0:T(8,128)(2,1)S(1)} %multiply_convert_fusion, bf16[1,896,2048]{2,1,0:T(8,128)(2,1)S(1)} %copy-done.10), kind=kOutput, calls=%fused_computation.25 | convolution fusion | flops 3525181440 | bytes 9322496 | tf_op jit(solution)/shard_map/dot_general | solution.py:145
  89.7 51.9 %while.15 = (s32[]{:T(128)}, f32[2,1024]{1,0:T(2,128)S(1)}, f32[2,1024]{1,0:T(2,128)S(1)}, f32[2,64,1024]{2,1,0:T(8,128)S(1)}, bf16[4,1024,64]{1,2,0:T(8,128)(2,...) while((s32[]{:T(128)}, f32[2,1024]{1,0:T(2,128)S(1)}, ...), condition=%wide.region_5.6_spmd.clone, body=%wide.region_2.5_spmd.clone.sunk | while | flops 554051584 | bytes 60424340 | solution.py:112
  89.8 5.4 %bitcast_reduce_fusion.2 = (f32[2,1024]{1,0:T(2,128)S(1)}, f32[1024,2,1024]{2,0,1:T(8,128)}) fusion(bf16[2,1024,64]{1,2,0:T(8,128)(2,1)S(1)} %get-tuple-element.201, bf16[4,1024,64]{1,2,0:T(8,128)(2,1)} %get-tuple-element.200, s32[]{:T(128)S(6)} %copy.61), kind=kOutput, calls=%fused_computation.4.clone.1 | convolution fusion | flops 272627712 | bytes 8790020 | tf_op jit(solution)/shard_map/while/body/eval_jaxpr/hqd,kd->hqk/dot_general | solution.py:94
  95.2 4.9 %fusion.64 = f32[2,1024]{1,0:T(2,128)S(1)} fusion(f32[1024,2,1024]{2,0,1:T(8,128)} %get-tuple-element.175, f32[2,1024]{1,0:T(2,128)S(1)} %fusion.63), kind=kLoop, calls=%fused_computation.7.clone.1 | loop fusion | flops 6289408 | bytes 8404992 | tf_op jit(solution)/shard_map/while/body/eval_jaxpr/reduce_sum | solution.py:102
  101.0 1.6 fusion.66
  102.6 5.4 %bitcast_reduce_fusion.2 = (f32[2,1024]{1,0:T(2,128)S(1)}, f32[1024,2,1024]{2,0,1:T(8,128)}) fusion(bf16[2,1024,64]{1,2,0:T(8,128)(2,1)S(1)} %get-tuple-element.201, bf16[4,1024,64]{1,2,0:T(8,128)(2,1)} %get-tuple-element.200, s32[]{:T(128)S(6)} %copy.61), kind=kOutput, calls=%fused_computation.4.clone.1 | convolution fusion | flops 272627712 | bytes 8790020 | tf_op jit(solution)/shard_map/while/body/eval_jaxpr/hqd,kd->hqk/dot_general | solution.py:94
  108.1 5.0 %fusion.64 = f32[2,1024]{1,0:T(2,128)S(1)} fusion(f32[1024,2,1024]{2,0,1:T(8,128)} %get-tuple-element.175, f32[2,1024]{1,0:T(2,128)S(1)} %fusion.63), kind=kLoop, calls=%fused_computation.7.clone.1 | loop fusion | flops 6289408 | bytes 8404992 | tf_op jit(solution)/shard_map/while/body/eval_jaxpr/reduce_sum | solution.py:102
  113.1 0.9 copy-done.1
  114.0 1.7 fusion.66
  115.7 5.4 %bitcast_reduce_fusion.2 = (f32[2,1024]{1,0:T(2,128)S(1)}, f32[1024,2,1024]{2,0,1:T(8,128)}) fusion(bf16[2,1024,64]{1,2,0:T(8,128)(2,1)S(1)} %get-tuple-element.201, bf16[4,1024,64]{1,2,0:T(8,128)(2,1)} %get-tuple-element.200, s32[]{:T(128)S(6)} %copy.61), kind=kOutput, calls=%fused_computation.4.clone.1 | convolution fusion | flops 272627712 | bytes 8790020 | tf_op jit(solution)/shard_map/while/body/eval_jaxpr/hqd,kd->hqk/dot_general | solution.py:94
  121.1 5.0 %fusion.64 = f32[2,1024]{1,0:T(2,128)S(1)} fusion(f32[1024,2,1024]{2,0,1:T(8,128)} %get-tuple-element.175, f32[2,1024]{1,0:T(2,128)S(1)} %fusion.63), kind=kLoop, calls=%fused_computation.7.clone.1 | loop fusion | flops 6289408 | bytes 8404992 | tf_op jit(solution)/shard_map/while/body/eval_jaxpr/reduce_sum | solution.py:102
  126.1 0.9 copy-done.1
  127.0 1.6 fusion.66
  128.7 5.4 %bitcast_reduce_fusion.2 = (f32[2,1024]{1,0:T(2,128)S(1)}, f32[1024,2,1024]{2,0,1:T(8,128)}) fusion(bf16[2,1024,64]{1,2,0:T(8,128)(2,1)S(1)} %get-tuple-element.201, bf16[4,1024,64]{1,2,0:T(8,128)(2,1)} %get-tuple-element.200, s32[]{:T(128)S(6)} %copy.61), kind=kOutput, calls=%fused_computation.4.clone.1 | convolution fusion | flops 272627712 | bytes 8790020 | tf_op jit(solution)/shard_map/while/body/eval_jaxpr/hqd,kd->hqk/dot_general | solution.py:94
  134.1 5.0 %fusion.64 = f32[2,1024]{1,0:T(2,128)S(1)} fusion(f32[1024,2,1024]{2,0,1:T(8,128)} %get-tuple-element.175, f32[2,1024]{1,0:T(2,128)S(1)} %fusion.63), kind=kLoop, calls=%fused_computation.7.clone.1 | loop fusion | flops 6289408 | bytes 8404992 | tf_op jit(solution)/shard_map/while/body/eval_jaxpr/reduce_sum | solution.py:102
  139.9 1.6 fusion.66
  141.7 0.8 copy.52
  142.6 2.0 %reshape.419 = bf16[4,30,2048]{2,1,0:T(8,128)(2,1)} reshape(bf16[120,2048]{1,0:T(8,128)(2,1)} %reduce-scatter.2.cloned.1.call-done) | data formatting | bytes 983040 | tf_op jit(solution)/shard_map/reshape | solution.py:151
  144.6 3.7 %all-to-all-start.1 = ((bf16[4,30,2048]{2,1,0:T(8,128)(2,1)}), bf16[4,30,2048]{2,1,0:T(8,128)(2,1)S(1)}, u32[]{:S(2)}, u32[]{:S(2)}) async-start(bf16[4,30,2048]{2,1,0:T(8,128)(2,1)} %reshape.419), calls=%async_computation.2 | async-start | bytes 1048576 | tf_op jit(solution)/shard_map/all_to_all | solution.py:150
  149.2 7.5 %all-to-all-done.1 = bf16[4,30,2048]{2,1,0:T(8,128)(2,1)S(1)} async-done(((bf16[4,30,2048]{2,1,0:T(8,128)(2,1)}), bf16[4,30,2048]{2,1,0:T(8,128)(2,1)S(1)}, u32[]{:S(2)}, u32[]{:S(2)}) %all-to-all-start.1) | async-done | bytes 491552 | tf_op jit(solution)/shard_map/all_to_all | solution.py:150
  156.9 0.8 gather_fusion.1
  158.0 2.0 %multiply_reduce_fusion = f32[48,2048]{1,0:T(8,128)S(1)} fusion(bf16[48,2,2048]{2,1,0:T(2,128)(2,1)S(1)} %gather.15, pred[48,2]{1,0:T(8,128)(4,1)S(1)} %copy.50, f32[48,2]{1,0:T(8,128)S(1)} %copy.47), kind=kLoop, calls=%fused_computation.32 | loop fusion | flops 688128 | bytes 786912 | tf_op jit(solution)/shard_map/reduce_sum | solution.py:159
  (97 shorter events, 9.5 us)
Async XLA Ops:
  7.2 20.2 %copy-start = (bf16[1024,256]{1,0:T(8,128)(2,1)S(1)}, bf16[1024,256]{1,0:T(8,128)(2,1)}, u32[]{:S(2)}) copy-start(bf16[1024,256]{1,0:T(8,128)(2,1)} %param.15) | copy-start | bytes 1572868
  7.2 64.5 %all-gather.3.cloned.1.call-start = ((), (), s32[]{:S(2)}) async-start(), calls=%async_computation.3 | async-start | bytes 4423680 | tf_op jit(solution)/shard_map/all_gather | solution.py:140
  12.2 15.7 %copy-start.6 = (f32[64]{0:T(128)S(1)}, f32[64]{0:T(128)}, u32[]{:S(2)}) copy-start(f32[64]{0:T(128)} %param.18) | copy-start | bytes 772
  12.5 27.4 %copy-start.3 = (bf16[1024,128]{1,0:T(8,128)(2,1)S(1)}, bf16[1024,128]{1,0:T(8,128)(2,1)}, u32[]{:S(2)}) copy-start(bf16[1024,128]{1,0:T(8,128)(2,1)} %param.14) | copy-start | bytes 786436
  26.2 13.9 %copy-start.4 = (bf16[1024,256]{1,0:T(8,128)(2,1)S(1)}, bf16[1024,256]{1,0:T(8,128)(2,1)}, u32[]{:S(2)}) copy-start(bf16[1024,256]{1,0:T(8,128)(2,1)} %param.16) | copy-start | bytes 1572868
  27.1 115.5 %reduce-scatter.2.cloned.1.call-start = ((), (), s32[]{:S(2)}) async-start(), calls=%async_computation.4 | async-start | bytes 4423680 | tf_op jit(solution)/shard_map/reduce_scatter | solution.py:144
  28.5 25.8 %copy-start.7 = (f32[64]{0:T(128)S(1)}, f32[64]{0:T(128)}, u32[]{:S(2)}) copy-start(f32[64]{0:T(128)} %param.17) | copy-start | bytes 772
  71.7 7.6 %copy-start.8 = (bf16[960,2048]{1,0:T(8,128)(2,1)S(1)}, bf16[960,2048]{1,0:T(8,128)(2,1)}, u32[]{:S(2)}) copy-start(bf16[960,2048]{1,0:T(8,128)(2,1)} %all-gather.3.cloned.1.call-done) | copy-start | bytes 11796484
  71.7 7.6 %copy-start.9 = (bf16[1,2048,896]{2,1,0:T(8,128)(2,1)S(1)}, bf16[1,2048,896]{2,1,0:T(8,128)(2,1)}, u32[]{:S(2)}) copy-start(bf16[1,2048,896]{2,1,0:T(8,128)(2,1)} %param.22) | copy-start | bytes 11010052
  79.3 4.5 %copy-start.10 = (bf16[1,896,2048]{2,1,0:T(8,128)(2,1)S(1)}, bf16[1,896,2048]{2,1,0:T(8,128)(2,1)}, u32[]{:S(2)}) copy-start(bf16[1,896,2048]{2,1,0:T(8,128)(2,1)} %param.24) | copy-start | bytes 11010052
  95.2 5.8 %copy-start.1 = (f32[1024,2,1024]{2,0,1:T(8,128)S(1)}, f32[1024,2,1024]{2,0,1:T(8,128)}, u32[]{:S(2)}) copy-start(f32[1024,2,1024]{2,0,1:T(8,128)} %get-tuple-element.175) | copy-start | bytes 25165828 | tf_op jit(solution)/shard_map/while
  108.1 5.9 %copy-start.1 = (f32[1024,2,1024]{2,0,1:T(8,128)S(1)}, f32[1024,2,1024]{2,0,1:T(8,128)}, u32[]{:S(2)}) copy-start(f32[1024,2,1024]{2,0,1:T(8,128)} %get-tuple-element.175) | copy-start | bytes 25165828 | tf_op jit(solution)/shard_map/while
  121.1 5.9 %copy-start.1 = (f32[1024,2,1024]{2,0,1:T(8,128)S(1)}, f32[1024,2,1024]{2,0,1:T(8,128)}, u32[]{:S(2)}) copy-start(f32[1024,2,1024]{2,0,1:T(8,128)} %get-tuple-element.175) | copy-start | bytes 25165828 | tf_op jit(solution)/shard_map/while
  134.1 5.9 %copy-start.1 = (f32[1024,2,1024]{2,0,1:T(8,128)S(1)}, f32[1024,2,1024]{2,0,1:T(8,128)}, u32[]{:S(2)}) copy-start(f32[1024,2,1024]{2,0,1:T(8,128)} %get-tuple-element.175) | copy-start | bytes 25165828 | tf_op jit(solution)/shard_map/while
  142.6 17.5 %copy-start.2 = (bf16[48,2048]{1,0:T(8,128)(2,1)S(1)}, bf16[48,2048]{1,0:T(8,128)(2,1)}, u32[]{:S(2)}) copy-start(bf16[48,2048]{1,0:T(8,128)(2,1)} %param.19) | copy-start | bytes 589828
  144.6 12.2 %all-to-all-start.1 = ((bf16[4,30,2048]{2,1,0:T(8,128)(2,1)}), bf16[4,30,2048]{2,1,0:T(8,128)(2,1)S(1)}, u32[]{:S(2)}, u32[]{:S(2)}) async-start(bf16[4,30,2048]{2,1,0:T(8,128)(2,1)} %reshape.419), calls=%async_computation.2 | async-start | bytes 1048576 | tf_op jit(solution)/shard_map/all_to_all | solution.py:150
  148.3 12.2 %copy-start.5 = (f32[2048]{0:T(1024)S(1)}, f32[2048]{0:T(1024)}, u32[]{:S(2)}) copy-start(f32[2048]{0:T(1024)} %param.25) | copy-start | bytes 24580
Sparse Core Ops, SparseCore 0:
  27.3 44.4 all-gather.2
  89.9 46.2 reduce-scatter.1
where the time goes:
time: 169 us; the launch traced here: 168 us
  matrix products  46.2 us (27%)
  blocking collectives  36.9 us (22%)
  other arithmetic  26.1 us (15%)
  waiting for transfers between devices  24.7 us (15%)
  local copies, waits for them, and re-layouts  15.7 us (9%)
  between operations  14.5 us (9%)
  starting transfers between devices  3.75 us (2%)
    dot_general x4, matrix products, sweep(): jnp.einsum('hqd,kd->hqk', rotated_queries, key_block, preferred_element_t...  21.6 us
    reduce_sum x4, other arithmetic, sweep(): row_total = row_total * shrink + jnp.sum(weights, axis=-1)  19.9 us
    all_gather x1, waiting for transfers between devices, shards(): lax.all_gather(arrived.reshape(-1, model_width), 'tp', axis=0, tiled=True)  17.2 us
    all_to_all x1, blocking collectives, shards(): lax.all_to_all(outgoing.reshape(experts, capacity, model_width), 'ep', sp...  13.6 us
    all_gather x1, blocking collectives, shards(): value_piece = lax.all_gather(value_cols, 'ep', axis=0, tiled=True)  13.1 us
    all_gather x1, blocking collectives, shards(): key_piece = lax.all_gather(rotated_keys, 'ep', axis=0, tiled=True)  10.1 us
    dot_general x1, matrix products, shards(): jnp.dot(shard_piece, up_weight[0], preferred_element_type=jnp.float32)  7.58 us
    all_to_all x1, waiting for transfers between devices, shards(): lax.all_to_all(expert_out.reshape(experts, capacity, model_width), 'ep',...  7.51 us
  transfers between devices with their start and end apart: 3, of which 2 were waited for; matrix products, arithmetic and copies ran while one was open for 32% of the time, Pallas kernels for 0%

commit v1 on v0

--- a/solution.py
+++ b/solution.py
@@ -80,8 +80,13 @@
         jnp.zeros((local_heads, seg_rows), jnp.float32),
         jnp.zeros((local_heads, head_size, seg_rows), jnp.float32),
     )
-    key_piece = lax.all_gather(rotated_keys, "ep", axis=0, tiled=True)
-    value_piece = lax.all_gather(value_cols, "ep", axis=0, tiled=True)
+    key_piece, value_piece = jnp.split(
+        lax.all_gather(
+            jnp.concatenate([rotated_keys, value_cols], axis=1), "ep", axis=0, tiled=True
+        ),
+        [rotated_keys.shape[1]],
+        axis=1,
+    )
     piece_rows = key_piece.shape[0]
     block_rows = math.gcd(piece_rows, 1024)
     key_blocks = key_piece.reshape(piece_rows // block_rows, block_rows, head_size)

time: 169 us -> 215 us (1.27)
  waiting for transfers between devices: 24.7 us -> 98.5 us
  blocking collectives: 36.9 us -> 13.5 us
  matrix products: 46.2 us -> 42.5 us
    reduce_scatter x1, waiting for transfers between devices: 0.01 us -> 48.4 us  [shards(): lax.psum_scatter(jnp.dot(hidden, down_weight[0], preferred_element_type=j...]
    all_gather x1, waiting for transfers between devices: 17.2 us -> 42.4 us  [shards(): lax.all_gather(arrived.reshape(-1, model_width), 'tp', axis=0, tiled=True)]
    all_gather x2 -> x0, blocking collectives: 23.3 us -> none  [the longest x1 13.1 us: shards(): value_piece = lax.all_gather(value_cols, 'ep', axis=0, tiled=True)]
    all_gather x0 -> x1, waiting for transfers between devices: none -> 7.67 us  [shards(): lax.all_gather(jnp.concatenate([rotated_keys, value_cols], axis=1), 'ep',...]
    all_to_all x1, waiting for transfers between devices: 7.51 us -> 0.01 us  [shards(): lax.all_to_all(expert_out.reshape(experts, capacity, model_width), 'ep',...]
    dot_general x4, matrix products: 21.6 us -> 18 us  [sweep(): jnp.einsum('hqd,kd->hqk', rotated_queries, key_block, preferred_element_t...]
  transfers between devices with their start and end apart: 3 -> 4, of which waited for: 2 -> 3; matrix products, arithmetic and copies ran while one was open for 32% -> 32% of each run, Pallas kernels for 0% -> 0%
where the time goes in v1:
time: 215 us
  waiting for transfers between devices  98.5 us (46%)
  matrix products  42.5 us (20%)
  other arithmetic  26.6 us (12%)
  local copies, waits for them, and re-layouts  15.5 us (7%)
  between operations  14.2 us (7%)
  blocking collectives  13.5 us (6%)
  starting transfers between devices  3.94 us (2%)
    reduce_scatter x1, waiting for transfers between devices, shards(): lax.psum_scatter(jnp.dot(hidden, down_weight[0], preferred_element_type=j...  48.4 us
    all_gather x1, waiting for transfers between devices, shards(): lax.all_gather(arrived.reshape(-1, model_width), 'tp', axis=0, tiled=True)  42.4 us
    reduce_sum x4, other arithmetic, sweep(): row_total = row_total * shrink + jnp.sum(weights, axis=-1)  19.7 us
    dot_general x4, matrix products, sweep(): jnp.einsum('hqd,kd->hqk', rotated_queries, key_block, preferred_element_t...  18 us
    all_to_all x1, blocking collectives, shards(): lax.all_to_all(outgoing.reshape(experts, capacity, model_width), 'ep', sp...  13.5 us
    all_gather x1, waiting for transfers between devices, shards(): lax.all_gather(jnp.concatenate([rotated_keys, value_cols], axis=1), 'ep',...  7.67 us
    dot_general x1, matrix products, shards(): jnp.dot(shard_piece, up_weight[0], preferred_element_type=jnp.float32)  7.58 us
    dot_general x4, matrix products, sweep(): jnp.einsum('hqk,kd->hdq', weights.astype(jnp.bfloat16), value_block, pref...  6.63 us
  transfers between devices with their start and end apart: 4, of which 3 were waited for; matrix products, arithmetic and copies ran while one was open for 32% of the time, Pallas kernels for 0%

profile of v1, /device:TPU:0, one launch (start us, length us, event | category | flops | bytes accessed | tf_op | source)
XLA Modules:
  0.0 214.9 jit_solution(11457365927766870493)
XLA Ops:
  8.9 0.9 scatter_custom_fusion
  9.8 2.4 %gather_fusion = bf16[120,2048]{1,0:T(8,128)(2,1)S(1)} fusion(bf16[48,2048]{1,0:T(8,128)(2,1)} %param.19, s32[1024]{0:T(1024)S(1)} %pad_clamp_fusion.1), kind=kCustom, calls=%fused_computation | custom fusion | bytes 983520 | tf_op jit(solution)/shard_map/jit(_take)/gather | solution.py:137
  12.6 13.5 %all_to_all.10 = bf16[4,30,2048]{2,1,0:T(8,128)(2,1)S(1)} all-to-all(bf16[4,30,2048]{2,1,0:T(8,128)(2,1)S(1)} %broadcast_select_fusion.2), channel_id=1, replica_groups=mesh['ep'=4,'tp'=8] {'ep'}, dimensions={0} | all-to-all | bytes 983040 | tf_op jit(solution)/shard_map/all_to_all | solution.py:138
  26.1 0.9 reshape.418
  29.3 42.4 %all-gather.5.cloned.1.call-done = bf16[960,2048]{1,0:T(8,128)(2,1)} async-done(((bf16[120,2048]{1,0:T(8,128)(2,1)}), bf16[960,2048]{1,0:T(8,128)(2,1)}) %all-gather.5.cloned.1.call-update) | async-done | bytes 3932176 | tf_op jit(solution)/shard_map/all_gather | solution.py:145
  71.6 7.6 %fusion.22 = f32[960,896]{1,0:T(8,128)S(1)} fusion(bf16[960,2048]{1,0:T(8,128)(2,1)} %all-gather.5.cloned.1.call-done, bf16[1,2048,896]{2,1,0:T(8,128)(2,1)} %param.23), kind=kOutput, calls=%fused_computation.27 | convolution fusion | flops 3523215360 | bytes 11042816 | tf_op jit(solution)/shard_map/dot_general | solution.py:147
  79.3 4.5 %multiply_convert_fusion = bf16[960,896]{1,0:T(8,128)(2,1)S(1)} fusion(f32[960,896]{1,0:T(8,128)S(1)} %fusion.22, bf16[960,2048]{1,0:T(8,128)(2,1)S(1)} %copy-done.9, bf16[1,2048,896]{2,1,0:T(8,128)(2,1)S(1)} %copy-done.10), kind=kOutput, calls=%fused_computation.31 | convolution fusion | flops 3528376320 | bytes 12763136 | tf_op jit(solution)/shard_map/dot_general | solution.py:146
  83.8 5.7 %convolution_convert_fusion = bf16[960,2048]{1,0:T(8,128)(2,1)} fusion(bf16[960,896]{1,0:T(8,128)(2,1)S(1)} %multiply_convert_fusion, bf16[1,896,2048]{2,1,0:T(8,128)(2,1)S(1)} %copy-done.11), kind=kOutput, calls=%fused_computation.25 | convolution fusion | flops 3525181440 | bytes 9322496 | tf_op jit(solution)/shard_map/dot_general | solution.py:150
  91.8 7.7 %all-gather.3.cloned.1.call-done = bf16[4096,128]{0,1:T(8,128)(2,1)} async-done(((bf16[1024,128]{0,1:T(8,128)(2,1)}), bf16[4096,128]{0,1:T(8,128)(2,1)}) %all-gather.3.cloned.1.call-update) | async-done | bytes 1048592 | tf_op jit(solution)/shard_map/all_gather | solution.py:84
  99.5 1.3 fusion.49
  100.8 48.4 %reduce-scatter.2.cloned.1.call-done = bf16[120,2048]{1,0:T(8,128)(2,1)} async-done(((bf16[960,2048]{1,0:T(8,128)(2,1)}), bf16[120,2048]{1,0:T(8,128)(2,1)}) %reduce-scatter.2.cloned.1.call-update) | async-done | bytes 491536 | tf_op jit(solution)/shard_map/reduce_scatter | solution.py:149
  149.2 2.0 reshape.419
  151.2 3.8 %all-to-all-start.1 = ((bf16[4,30,2048]{2,1,0:T(8,128)(2,1)}), bf16[4,30,2048]{2,1,0:T(8,128)(2,1)S(1)}, u32[]{:S(2)}, u32[]{:S(2)}) async-start(bf16[4,30,2048]{2,1,0:T(8,128)(2,1)} %reshape.419), calls=%async_computation.2 | async-start | bytes 1048576 | tf_op jit(solution)/shard_map/all_to_all | solution.py:155
  155.1 47.9 %while.15 = (s32[]{:T(128)}, f32[2,1024]{1,0:T(2,128)S(1)}, f32[2,1024]{1,0:T(2,128)S(1)}, f32[2,64,1024]{2,1,0:T(8,128)S(1)}, bf16[4,1024,64]{1,2,0:T(8,128)(2,...) while((s32[]{:T(128)}, f32[2,1024]{1,0:T(2,128)S(1)}, ...), condition=%wide.region_5.6_spmd.clone, body=%wide.region_2.5_spmd.clone.sunk | while | flops 554051584 | bytes 60424340 | solution.py:117
  155.1 4.5 %bitcast_reduce_fusion.2 = (f32[2,1024]{1,0:T(2,128)S(1)}, f32[1024,2,1024]{2,0,1:T(8,128)}) fusion(bf16[2,1024,64]{1,2,0:T(8,128)(2,1)S(1)} %get-tuple-element.205, bf16[4,1024,64]{1,2,0:T(8,128)(2,1)S(1)} %get-tuple-element.204, s32[]{:T(128)S(6)} %copy.66), kind=kOutput, calls=%fused_computation.4.clone.1 | convolution fusion | flops 272627712 | bytes 8790020 | tf_op jit(solution)/shard_map/while/body/eval_jaxpr/hqd,kd->hqk/dot_general | solution.py:99
  159.6 4.9 %fusion.65 = f32[2,1024]{1,0:T(2,128)S(1)} fusion(f32[1024,2,1024]{2,0,1:T(8,128)} %get-tuple-element.179, f32[2,1024]{1,0:T(2,128)S(1)} %fusion.64), kind=kLoop, calls=%fused_computation.7.clone.1 | loop fusion | flops 6289408 | bytes 8404992 | tf_op jit(solution)/shard_map/while/body/eval_jaxpr/reduce_sum | solution.py:107
  164.5 0.8 copy-done.1
  165.3 1.7 fusion.67
  167.0 4.5 %bitcast_reduce_fusion.2 = (f32[2,1024]{1,0:T(2,128)S(1)}, f32[1024,2,1024]{2,0,1:T(8,128)}) fusion(bf16[2,1024,64]{1,2,0:T(8,128)(2,1)S(1)} %get-tuple-element.205, bf16[4,1024,64]{1,2,0:T(8,128)(2,1)S(1)} %get-tuple-element.204, s32[]{:T(128)S(6)} %copy.66), kind=kOutput, calls=%fused_computation.4.clone.1 | convolution fusion | flops 272627712 | bytes 8790020 | tf_op jit(solution)/shard_map/while/body/eval_jaxpr/hqd,kd->hqk/dot_general | solution.py:99
  171.6 4.9 %fusion.65 = f32[2,1024]{1,0:T(2,128)S(1)} fusion(f32[1024,2,1024]{2,0,1:T(8,128)} %get-tuple-element.179, f32[2,1024]{1,0:T(2,128)S(1)} %fusion.64), kind=kLoop, calls=%fused_computation.7.clone.1 | loop fusion | flops 6289408 | bytes 8404992 | tf_op jit(solution)/shard_map/while/body/eval_jaxpr/reduce_sum | solution.py:107
  177.3 1.7 fusion.67
  179.0 4.5 %bitcast_reduce_fusion.2 = (f32[2,1024]{1,0:T(2,128)S(1)}, f32[1024,2,1024]{2,0,1:T(8,128)}) fusion(bf16[2,1024,64]{1,2,0:T(8,128)(2,1)S(1)} %get-tuple-element.205, bf16[4,1024,64]{1,2,0:T(8,128)(2,1)S(1)} %get-tuple-element.204, s32[]{:T(128)S(6)} %copy.66), kind=kOutput, calls=%fused_computation.4.clone.1 | convolution fusion | flops 272627712 | bytes 8790020 | tf_op jit(solution)/shard_map/while/body/eval_jaxpr/hqd,kd->hqk/dot_general | solution.py:99
  183.5 4.9 %fusion.65 = f32[2,1024]{1,0:T(2,128)S(1)} fusion(f32[1024,2,1024]{2,0,1:T(8,128)} %get-tuple-element.179, f32[2,1024]{1,0:T(2,128)S(1)} %fusion.64), kind=kLoop, calls=%fused_computation.7.clone.1 | loop fusion | flops 6289408 | bytes 8404992 | tf_op jit(solution)/shard_map/while/body/eval_jaxpr/reduce_sum | solution.py:107
  188.5 0.8 copy-done.1
  189.3 1.7 fusion.67
  191.0 4.5 %bitcast_reduce_fusion.2 = (f32[2,1024]{1,0:T(2,128)S(1)}, f32[1024,2,1024]{2,0,1:T(8,128)}) fusion(bf16[2,1024,64]{1,2,0:T(8,128)(2,1)S(1)} %get-tuple-element.205, bf16[4,1024,64]{1,2,0:T(8,128)(2,1)S(1)} %get-tuple-element.204, s32[]{:T(128)S(6)} %copy.66), kind=kOutput, calls=%fused_computation.4.clone.1 | convolution fusion | flops 272627712 | bytes 8790020 | tf_op jit(solution)/shard_map/while/body/eval_jaxpr/hqd,kd->hqk/dot_general | solution.py:99
  195.5 4.9 %fusion.65 = f32[2,1024]{1,0:T(2,128)S(1)} fusion(f32[1024,2,1024]{2,0,1:T(8,128)} %get-tuple-element.179, f32[2,1024]{1,0:T(2,128)S(1)} %fusion.64), kind=kLoop, calls=%fused_computation.7.clone.1 | loop fusion | flops 6289408 | bytes 8404992 | tf_op jit(solution)/shard_map/while/body/eval_jaxpr/reduce_sum | solution.py:107
  200.4 0.8 copy-done.1
  201.2 1.7 fusion.67
  203.0 0.8 copy.52
  204.0 0.8 gather_fusion.1
  205.1 2.1 multiply_reduce_fusion
  (101 shorter events, 8.9 us)
Async XLA Ops:
  7.2 83.7 %copy-start = (f32[384,2]{0,1:T(2,128)S(1)}, f32[384,2]{0,1:T(2,128)}, u32[]{:S(2)}) copy-start(f32[384,2]{0,1:T(2,128)} %param.21) | copy-start | bytes 9220
  7.2 64.5 %all-gather.5.cloned.1.call-start = ((), (), s32[]{:S(2)}) async-start(), calls=%async_computation.4 | async-start | bytes 4423680 | tf_op jit(solution)/shard_map/all_gather | solution.py:145
  9.8 17.4 %copy-start.4 = (bf16[1024,256]{1,0:T(8,128)(2,1)S(1)}, bf16[1024,256]{1,0:T(8,128)(2,1)}, u32[]{:S(2)}) copy-start(bf16[1024,256]{1,0:T(8,128)(2,1)} %param.16) | copy-start | bytes 1572868
  9.8 17.4 %copy-start.5 = (bf16[1024,256]{1,0:T(8,128)(2,1)S(1)}, bf16[1024,256]{1,0:T(8,128)(2,1)}, u32[]{:S(2)}) copy-start(bf16[1024,256]{1,0:T(8,128)(2,1)} %param.15) | copy-start | bytes 1572868
  12.2 15.6 %copy-start.7 = (f32[64]{0:T(128)S(1)}, f32[64]{0:T(128)}, u32[]{:S(2)}) copy-start(f32[64]{0:T(128)} %param.18) | copy-start | bytes 772
  27.1 72.4 %all-gather.3.cloned.1.call-start = ((), (), s32[]{:S(2)}) async-start(), calls=%async_computation.3 | async-start | bytes 1310720 | tf_op jit(solution)/shard_map/all_gather | solution.py:84
  29.2 120.0 %reduce-scatter.2.cloned.1.call-start = ((), (), s32[]{:S(2)}) async-start(), calls=%async_computation.5 | async-start | bytes 4423680 | tf_op jit(solution)/shard_map/reduce_scatter | solution.py:149
  71.6 7.6 %copy-start.9 = (bf16[960,2048]{1,0:T(8,128)(2,1)S(1)}, bf16[960,2048]{1,0:T(8,128)(2,1)}, u32[]{:S(2)}) copy-start(bf16[960,2048]{1,0:T(8,128)(2,1)} %all-gather.5.cloned.1.call-done) | copy-start | bytes 11796484
  71.6 7.6 %copy-start.10 = (bf16[1,2048,896]{2,1,0:T(8,128)(2,1)S(1)}, bf16[1,2048,896]{2,1,0:T(8,128)(2,1)}, u32[]{:S(2)}) copy-start(bf16[1,2048,896]{2,1,0:T(8,128)(2,1)} %param.22) | copy-start | bytes 11010052
  79.3 4.5 %copy-start.11 = (bf16[1,896,2048]{2,1,0:T(8,128)(2,1)S(1)}, bf16[1,896,2048]{2,1,0:T(8,128)(2,1)}, u32[]{:S(2)}) copy-start(bf16[1,896,2048]{2,1,0:T(8,128)(2,1)} %param.24) | copy-start | bytes 11010052
  89.5 0.9 copy-start.3
  89.5 2.0 copy-start.8
  151.2 52.6 %all-to-all-start.1 = ((bf16[4,30,2048]{2,1,0:T(8,128)(2,1)}), bf16[4,30,2048]{2,1,0:T(8,128)(2,1)S(1)}, u32[]{:S(2)}, u32[]{:S(2)}) async-start(bf16[4,30,2048]{2,1,0:T(8,128)(2,1)} %reshape.419), calls=%async_computation.2 | async-start | bytes 1048576 | tf_op jit(solution)/shard_map/all_to_all | solution.py:155
  159.6 5.8 %copy-start.1 = (f32[1024,2,1024]{2,0,1:T(8,128)S(1)}, f32[1024,2,1024]{2,0,1:T(8,128)}, u32[]{:S(2)}) copy-start(f32[1024,2,1024]{2,0,1:T(8,128)} %get-tuple-element.179) | copy-start | bytes 25165828 | tf_op jit(solution)/shard_map/while
  171.5 5.8 %copy-start.1 = (f32[1024,2,1024]{2,0,1:T(8,128)S(1)}, f32[1024,2,1024]{2,0,1:T(8,128)}, u32[]{:S(2)}) copy-start(f32[1024,2,1024]{2,0,1:T(8,128)} %get-tuple-element.179) | copy-start | bytes 25165828 | tf_op jit(solution)/shard_map/while
  183.5 5.8 %copy-start.1 = (f32[1024,2,1024]{2,0,1:T(8,128)S(1)}, f32[1024,2,1024]{2,0,1:T(8,128)}, u32[]{:S(2)}) copy-start(f32[1024,2,1024]{2,0,1:T(8,128)} %get-tuple-element.179) | copy-start | bytes 25165828 | tf_op jit(solution)/shard_map/while
  195.5 5.8 %copy-start.1 = (f32[1024,2,1024]{2,0,1:T(8,128)S(1)}, f32[1024,2,1024]{2,0,1:T(8,128)}, u32[]{:S(2)}) copy-start(f32[1024,2,1024]{2,0,1:T(8,128)} %get-tuple-element.179) | copy-start | bytes 25165828 | tf_op jit(solution)/shard_map/while
  202.9 4.2 %copy-start.2 = (bf16[48,2048]{1,0:T(8,128)(2,1)S(1)}, bf16[48,2048]{1,0:T(8,128)(2,1)}, u32[]{:S(2)}) copy-start(bf16[48,2048]{1,0:T(8,128)(2,1)} %param.19) | copy-start | bytes 589828
  203.0 4.6 %copy-start.6 = (f32[2048]{0:T(1024)S(1)}, f32[2048]{0:T(1024)}, u32[]{:S(2)}) copy-start(f32[2048]{0:T(1024)} %param.25) | copy-start | bytes 24580
Sparse Core Ops, SparseCore 0:
  27.2 44.4 all-gather.4
  74.1 25.3 all-gather.2
  101.8 47.3 reduce-scatter.1
